TPU v7x, 32 devices: a whole 2x2x4 slice. The times are simulated.
32 devices in a mesh: fs: 4 (over y, x), tp: 8 (over z, core).
Axes of the slice: x: 2, y: 2, z: 4, core: 2. Of those that a mesh axis runs over, the one named last changes fastest.
Arguments:
- saved_inputs: bfloat16 [2688, 4096], P('fs', 'tp'), may hold values from -6 to 6
- proj_cotangent: bfloat16 [2688, 4096], P('fs', 'tp'), may hold values from -0.115722656 to 0.115722656
- saved_hidden: bfloat16 [2688, 4096], P('fs', 'tp'), may hold values from -6 to 6
- out_cotangent: bfloat16 [2688, 4096], P('fs', 'tp'), may hold values from -0.115722656 to 0.115722656
- factors: bfloat16 [2, 4096, 128], replicated, may hold values from -0.46875 to 0.46875
- w_proj: float32 [4096, 4096], P('fs', 'tp'), may hold values from -0.09375 to 0.09375
- w_out: float32 [4096, 4096], P('tp', 'fs'), may hold values from -0.09375 to 0.09375
- moment_first: float32 [2, 128, 4096], P(None, None, 'tp'), may hold values from -1.8 to 1.8
- moment_second: float32 [2, 128, 4096], P(None, None, 'tp'), may hold values from 0.05 to 1
Outputs:
- proj_next: float32 [4096, 4096], P('fs', 'tp')
- out_next: float32 [4096, 4096], P('tp', 'fs')
- proj_copy: bfloat16 [4096, 4096], P(None, 'tp')
- out_copy: bfloat16 [4096, 4096], P('tp')
- first_next: float32 [2, 128, 4096], P(None, None, 'tp')
- second_next: float32 [2, 128, 4096], P(None, None, 'tp')
All inputs are finite; a program needn't handle non-finite values.
Results may differ from a plain program's by a relative error of at most 0.001.
Values may be sent and summed in bfloat16 or wider, within the bound.
A program may use at most 64 MiB of HBM per device.

v0:
```python
import jax
import jax.numpy as jnp
from jax import lax
from jax.sharding import PartitionSpec as P

beta_first = 0.9
beta_second = 0.95
learn_rate = 0.02
epsilon = 1e-06


def over_tokens(left_rows, right_rows, precise):
    return lax.dot_general(
        left_rows,
        right_rows,
        (((0,), (0,)), ((), ())),
        preferred_element_type=jnp.float32,
        precision=precise,
    )


def body(
    saved_inputs,
    proj_cotangent,
    saved_hidden,
    out_cotangent,
    factors,
    w_proj,
    w_out,
    moment_first,
    moment_second,
):
    highest = lax.Precision.HIGHEST
    fs_count = lax.axis_size("fs")
    tp_count = lax.axis_size("tp")
    d_model = factors.shape[1]
    hidden_width = proj_cotangent.shape[1]
    fs_rows = d_model // fs_count
    tp_feats = saved_inputs.shape[1]
    own_rows = lax.dynamic_slice_in_dim(factors, lax.axis_index("fs") * fs_rows, fs_rows, 1).astype(
        jnp.float32
    )
    own_feats = lax.dynamic_slice_in_dim(factors, lax.axis_index("tp") * tp_feats, tp_feats, 1)
    proj_rows = jnp.dot(saved_inputs, own_feats[0], preferred_element_type=jnp.float32)
    out_rows = jnp.dot(out_cotangent, own_feats[1], preferred_element_type=jnp.float32)
    proj_rows, out_rows = lax.psum((proj_rows, out_rows), "tp")
    partial_sums = jnp.stack(
        [
            over_tokens(proj_rows, proj_cotangent.astype(jnp.float32), highest),
            over_tokens(out_rows, saved_hidden.astype(jnp.float32), highest),
        ]
    )
    small_grads = lax.psum(partial_sums, "fs")
    first_next = beta_first * moment_first + (1.0 - beta_first) * small_grads
    second_next = beta_second * moment_second + (1.0 - beta_second) * small_grads * small_grads
    direction = first_next / (jnp.sqrt(second_next) + epsilon)
    update_full = jnp.einsum("kdr,kre->kde", own_rows, direction, precision=highest)
    squares = lax.psum(jnp.sum(update_full * update_full, axis=(1, 2)), ("fs", "tp"))
    norm_scale = lax.rsqrt(squares / (d_model * hidden_width * tp_count) + epsilon)
    stepped = update_full * norm_scale[:, None, None]
    proj_next = w_proj - learn_rate * stepped[0]
    out_next = w_out - learn_rate * stepped[1].T
    proj_copy, out_copy = (
        lax.all_gather(proj_next.astype(jnp.bfloat16), "fs", axis=0, tiled=True),
        lax.all_gather(out_next.astype(jnp.bfloat16), "fs", axis=1, tiled=True),
    )
    return (proj_next, out_next, proj_copy, out_copy, first_next, second_next)


def solution(mesh):
    placed = (
        P("fs", "tp"),
        P("fs", "tp"),
        P("fs", "tp"),
        P("fs", "tp"),
        P(),
        P("fs", "tp"),
        P("tp", "fs"),
        P(None, None, "tp"),
        P(None, None, "tp"),
    )
    return jax.shard_map(
        body,
        mesh=mesh,
        in_specs=placed,
        out_specs=(
            P("fs", "tp"),
            P("tp", "fs"),
            P(None, "tp"),
            P("tp", None),
            P(None, None, "tp"),
            P(None, None, "tp"),
        ),
        check_vma=False,
    )
```

profile of v0, /device:TPU:0, one launch (start us, length us, event | category | flops | bytes accessed | tf_op | source)
XLA Modules:
  0.0 292.3 jit_solution(14841451723777137700)
XLA Ops:
  7.2 1.5 copy-done
  8.8 2.3 convolution_bitcast_fusion.1
  11.1 2.2 convolution_bitcast_fusion
  13.3 0.0 all-reduce.4.cloned.1.call-start
  13.3 60.8 %all-reduce.6.cloned.1.call-done = (f32[672,128]{0,1:T(8,128)}, f32[672,128]{0,1:T(8,128)}) async-done(((f32[672,128]{0,1:T(8,128)}, f32[672,128]{0,1:T(8,128)}), (f32[672,128]{0,1:T(8,128)}, f32[672,128]{0,1:T(8,128)})) %all-reduce.6.cloned.1.call-update) | async-done | bytes 688144 | tf_op jit(solution)/shard_map/psum | solution.py:46
  74.1 1.5 convolution_bitcast_fusion.2
  75.6 1.5 convolution_bitcast_fusion.3
  77.1 0.8 pad_maximum_fusion
  77.9 0.0 all-gather.5.cloned.1.call-start
  78.0 2.9 copy.15
  80.9 41.7 %all-reduce.4.cloned.1.call-done = f32[2,128,512]{2,1,0:T(8,128)} async-done(((f32[2,128,512]{2,1,0:T(8,128)}), f32[2,128,512]{2,1,0:T(8,128)}) %all-reduce.4.cloned.1.call-update) | async-done | bytes 524304 | tf_op jit(solution)/shard_map/psum | solution.py:53
  122.6 1.6 fusion.4
  124.2 4.0 %multiply_reduce_fusion = (f32[2]{0:T(128)S(1)}, f32[2,1024,512]{2,1,0:T(8,128)}) fusion(f32[2,128,512]{2,1,0:T(8,128)S(1)} %get-tuple-element.32, f32[2,128,512]{2,1,0:T(8,128)S(1)} %get-tuple-element.33, bf16[2,4096,128]{2,1,0:T(8,128)(2,1)S(1)} %copy-done, s32[]{:T(128)S(6)} %select_n.6), kind=kOutput, calls=%fused_computation | convolution fusion | flops 1612972032 | bytes 5767180 | tf_op jit(solution)/shard_map/kdr,kre->kde/dot_general | solution.py:57
  128.2 39.2 %psum.31 = f32[2]{0:T(128)S(1)} all-reduce(f32[2]{0:T(128)S(1)} %get-tuple-element.20), channel_id=1, replica_groups=mesh['fs'=4,'tp'=8] {'fs','tp'}, use_global_device_ids=true, to_apply=%region_4.0 | all-reduce | flops 2 | bytes 16 | tf_op jit(solution)/shard_map/psum | solution.py:58
  167.4 3.1 %broadcast_multiply_fusion = f32[2,1024,512]{2,1,0:T(8,128)S(1)} fusion(f32[2,1024,512]{2,1,0:T(8,128)} %get-tuple-element.21, f32[2]{0:T(128)S(1)} %add_rsqrt_fusion), kind=kLoop, calls=%fused_computation.7 | loop fusion | flops 1048576 | bytes 8388616 | tf_op jit(solution)/shard_map/mul | solution.py:60
  170.6 2.6 fusion.15
  173.2 0.4 copy-done.1
  173.6 0.0 all-gather.3.cloned.1.call-start
  173.6 4.5 %fusion.17 = (bf16[1024,512]{1,0:T(8,128)(2,1)}, f32[1024,512]{1,0:T(8,128)}) fusion(f32[1024,512]{1,0:T(8,128)} %param.14, f32[2,1024,512]{2,1,0:T(8,128)} %copy-done.1), kind=kLoop, calls=%fused_computation.30 | loop fusion | flops 1572864 | bytes 7340032 | tf_op jit(solution)/shard_map/convert_element_type | solution.py:64
  178.1 2.9 copy.16
  181.0 46.0 %all-gather.5.cloned.1.call-done = bf16[512,4096]{0,1:T(8,128)(2,1)} async-done(((bf16[512,1024]{0,1:T(8,128)(2,1)}), bf16[512,4096]{0,1:T(8,128)(2,1)}) %all-gather.5.cloned.1.call-update) | async-done | bytes 4194320 | tf_op jit(solution)/shard_map/all_gather | solution.py:65
  227.0 6.3 %copy.17 = bf16[512,4096]{1,0:T(8,128)(2,1)} copy(bf16[512,4096]{0,1:T(8,128)(2,1)} %all-gather.5.cloned.1.call-done) | data formatting | bytes 8388608
  233.3 48.0 %all-gather.3.cloned.1.call-done = bf16[4096,512]{1,0:T(8,128)(2,1)} async-done(((bf16[1024,512]{1,0:T(8,128)(2,1)}), bf16[4096,512]{1,0:T(8,128)(2,1)}) %all-gather.3.cloned.1.call-update) | async-done | bytes 4194320 | tf_op jit(solution)/shard_map/all_gather | solution.py:64
  281.3 4.5 %copy.22 = bf16[4096,512]{1,0:T(8,128)(2,1)} copy(bf16[4096,512]{1,0:T(8,128)(2,1)} %all-gather.3.cloned.1.call-done) | data formatting | bytes 8388608
  (18 shorter events, 0.1 us)
Async XLA Ops:
  7.2 1.6 copy-start
  7.2 66.9 %copy-start.5 = (bf16[672,512]{1,0:T(8,128)(2,1)S(1)}, bf16[672,512]{1,0:T(8,128)(2,1)}, u32[]{:S(2)}) copy-start(bf16[672,512]{1,0:T(8,128)(2,1)} %param.11) | copy-start | bytes 2064388
  7.2 66.9 %all-reduce.6.cloned.1.call-start = ((), (), s32[]{:S(2)}) async-start(), calls=%async_computation.3 | async-start | bytes 1572864 | tf_op jit(solution)/shard_map/psum | solution.py:46
  8.8 66.8 %copy-start.6 = (bf16[672,512]{1,0:T(8,128)(2,1)S(1)}, bf16[672,512]{1,0:T(8,128)(2,1)}, u32[]{:S(2)}) copy-start(bf16[672,512]{1,0:T(8,128)(2,1)} %param.10) | copy-start | bytes 2064388
  13.3 109.3 %all-reduce.4.cloned.1.call-start = ((), (), s32[]{:S(2)}) async-start(), calls=%async_computation | async-start | bytes 1048576 | tf_op jit(solution)/shard_map/psum | solution.py:53
  77.9 149.1 %all-gather.5.cloned.1.call-start = ((), (), s32[]{:S(2)}) async-start(), calls=%async_computation.2 | async-start | bytes 5242880 | tf_op jit(solution)/shard_map/all_gather | solution.py:65
  124.2 4.0 %copy-start.3 = (f32[2,128,512]{2,1,0:T(8,128)}, f32[2,128,512]{2,1,0:T(8,128)S(1)}, u32[]{:S(2)}) copy-start(f32[2,128,512]{2,1,0:T(8,128)S(1)} %get-tuple-element.33) | copy-start | bytes 1572868
  124.2 4.0 %copy-start.4 = (f32[2,128,512]{2,1,0:T(8,128)}, f32[2,128,512]{2,1,0:T(8,128)S(1)}, u32[]{:S(2)}) copy-start(f32[2,128,512]{2,1,0:T(8,128)S(1)} %get-tuple-element.32) | copy-start | bytes 1572868
  167.4 3.1 %copy-start.2 = (f32[512,1024]{0,1:T(8,128)S(1)}, f32[512,1024]{0,1:T(8,128)}, u32[]{:S(2)}) copy-start(f32[512,1024]{0,1:T(8,128)} %copy.15) | copy-start | bytes 6291460
  170.6 3.0 %copy-start.1 = (f32[2,1024,512]{2,1,0:T(8,128)}, f32[2,1024,512]{2,1,0:T(8,128)S(1)}, u32[]{:S(2)}) copy-start(f32[2,1024,512]{2,1,0:T(8,128)S(1)} %broadcast_multiply_fusion) | copy-start | bytes 12582916
  173.6 107.8 %all-gather.3.cloned.1.call-start = ((), (), s32[]{:S(2)}) async-start(), calls=%async_computation.1 | async-start | bytes 5242880 | tf_op jit(solution)/shard_map/all_gather | solution.py:64
Sparse Core Ops, SparseCore 0:
  13.4 60.6 all-reduce.5
  78.1 44.4 all-reduce.3
  173.7 53.2 all-gather.4
  228.7 52.5 all-gather.2
where the time goes:
time: 293 us; the launch traced here: 292 us
  waiting for transfers between devices  197 us (67%)
  blocking collectives  39.2 us (13%)
  local copies, waits for them, and re-layouts  18.5 us (6%)
  between operations  13.9 us (5%)
  other arithmetic  12.6 us (4%)
  matrix products  11.4 us (4%)
    psum x1, waiting for transfers between devices, body(): proj_rows, out_rows = lax.psum((proj_rows, out_rows), 'tp')  60.8 us
    all_gather x1, waiting for transfers between devices, body(): lax.all_gather(proj_next.astype(jnp.bfloat16), 'fs', axis=0, tiled=True)  48 us
    all_gather x1, waiting for transfers between devices, body(): lax.all_gather(out_next.astype(jnp.bfloat16), 'fs', axis=1, tiled=True)  46 us
    psum x1, waiting for transfers between devices, body(): small_grads = lax.psum(partial_sums, 'fs')  41.7 us
    psum x1, blocking collectives, body(): lax.psum(jnp.sum(update_full * update_full, axis=(1, 2)), ('fs', 'tp'))  39.2 us
    unnamed x18, local copies, waits for them, and re-layouts  18.5 us
  transfers between devices with their start and end apart: 4, of which 4 were waited for; matrix products, arithmetic and copies ran while one was open for 6% of the time, Pallas kernels for 0%

commit v1 on v0

--- a/solution.py
+++ b/solution.py
@@ -55,7 +55,7 @@
     second_next = beta_second * moment_second + (1.0 - beta_second) * small_grads * small_grads
     direction = first_next / (jnp.sqrt(second_next) + epsilon)
     update_full = jnp.einsum("kdr,kre->kde", own_rows, direction, precision=highest)
-    squares = lax.psum(jnp.sum(update_full * update_full, axis=(1, 2)), ("fs", "tp"))
+    squares = lax.psum(lax.psum(jnp.sum(update_full * update_full, axis=(1, 2)), "tp"), "fs")
     norm_scale = lax.rsqrt(squares / (d_model * hidden_width * tp_count) + epsilon)
     stepped = update_full * norm_scale[:, None, None]
     proj_next = w_proj - learn_rate * stepped[0]

time: 293 us -> 278 us (0.949)
  blocking collectives: 39.2 us -> 24.7 us
    psum x1 -> x2, blocking collectives: 39.2 us -> 24.7 us  [the longest x1 15.8 us: body(): lax.psum(jnp.sum(update_full * update_full, axis=(1, 2)), 'tp')]
    all_gather x1, waiting for transfers between devices: 46 us -> 42.3 us  [body(): lax.all_gather(out_next.astype(jnp.bfloat16), 'fs', axis=1, tiled=True)]
  transfers between devices with their start and end apart: 4 -> 4, of which waited for: 4 -> 4; matrix products, arithmetic and copies ran while one was open for 6% -> 5% of each run, Pallas kernels for 0% -> 0%
where the time goes in v1:
time: 278 us; the launch traced here: 277 us
  waiting for transfers between devices  196 us (71%)
  blocking collectives  24.7 us (9%)
  local copies, waits for them, and re-layouts  18.7 us (7%)
  between operations  13.9 us (5%)
  other arithmetic  12.6 us (5%)
  matrix products  11.4 us (4%)
    psum x1, waiting for transfers between devices, body(): proj_rows, out_rows = lax.psum((proj_rows, out_rows), 'tp')  60.8 us
    all_gather x1, waiting for transfers between devices, body(): lax.all_gather(proj_next.astype(jnp.bfloat16), 'fs', axis=0, tiled=True)  48 us
    psum x1, waiting for transfers between devices, body(): small_grads = lax.psum(partial_sums, 'fs')  44.6 us
    all_gather x1, waiting for transfers between devices, body(): lax.all_gather(out_next.astype(jnp.bfloat16), 'fs', axis=1, tiled=True)  42.3 us
    unnamed x18, local copies, waits for them, and re-layouts  18.7 us
    psum x1, blocking collectives, body(): lax.psum(jnp.sum(update_full * update_full, axis=(1, 2)), 'tp')  15.8 us
    psum x1, blocking collectives, body(): lax.psum(lax.psum(jnp.sum(update_full * update_full, axis=(1, 2)), 'tp'),...  8.89 us
  transfers between devices with their start and end apart: 4, of which 4 were waited for; matrix products, arithmetic and copies ran while one was open for 5% of the time, Pallas kernels for 0%

profile of v1, /device:TPU:0, one launch (start us, length us, event | category | flops | bytes accessed | tf_op | source)
XLA Modules:
  0.0 277.2 jit_solution(2148853521325239321)
XLA Ops:
  7.2 1.5 copy-done
  8.8 2.3 convolution_bitcast_fusion.1
  11.1 2.2 convolution_bitcast_fusion
  13.3 0.0 all-reduce.4.cloned.1.call-start
  13.3 60.8 %all-reduce.6.cloned.1.call-done = (f32[672,128]{0,1:T(8,128)}, f32[672,128]{0,1:T(8,128)}) async-done(((f32[672,128]{0,1:T(8,128)}, f32[672,128]{0,1:T(8,128)}), (f32[672,128]{0,1:T(8,128)}, f32[672,128]{0,1:T(8,128)})) %all-reduce.6.cloned.1.call-update) | async-done | bytes 688144 | tf_op jit(solution)/shard_map/psum | solution.py:46
  74.1 1.5 convolution_bitcast_fusion.2
  75.6 1.5 convolution_bitcast_fusion.3
  77.1 0.8 pad_maximum_fusion
  78.0 44.6 %all-reduce.4.cloned.1.call-done = f32[2,128,512]{2,1,0:T(8,128)} async-done(((f32[2,128,512]{2,1,0:T(8,128)}), f32[2,128,512]{2,1,0:T(8,128)}) %all-reduce.4.cloned.1.call-update) | async-done | bytes 524304 | tf_op jit(solution)/shard_map/psum | solution.py:53
  122.6 1.6 fusion.4
  124.2 4.0 %multiply_reduce_fusion = (f32[2]{0:T(128)S(1)}, f32[2,1024,512]{2,1,0:T(8,128)}) fusion(f32[2,128,512]{2,1,0:T(8,128)S(1)} %get-tuple-element.32, f32[2,128,512]{2,1,0:T(8,128)S(1)} %get-tuple-element.33, bf16[2,4096,128]{2,1,0:T(8,128)(2,1)S(1)} %copy-done, s32[]{:T(128)S(6)} %select_n.6), kind=kOutput, calls=%fused_computation | convolution fusion | flops 1612972032 | bytes 5767180 | tf_op jit(solution)/shard_map/kdr,kre->kde/dot_general | solution.py:57
  128.2 15.8 %psum.38 = f32[2]{0:T(128)S(1)} all-reduce(f32[2]{0:T(128)S(1)} %get-tuple-element.20), channel_id=1, replica_groups=mesh['fs'=4,'tp'=8] {'tp'}, use_global_device_ids=true, to_apply=%region_4.0 | all-reduce | flops 2 | bytes 16 | tf_op jit(solution)/shard_map/psum | solution.py:58
  144.0 2.9 %copy.15 = f32[512,1024]{0,1:T(8,128)} copy(f32[512,1024]{1,0:T(8,128)} %param.15) | data formatting | bytes 4194304 | tf_op args[6]
  146.9 8.9 %psum.39 = f32[2]{0:T(128)S(1)} all-reduce(f32[2]{0:T(128)S(1)} %psum.38), channel_id=1, replica_groups=mesh['fs'=4,'tp'=8] {'fs'}, use_global_device_ids=true, to_apply=%region_5.0 | all-reduce | flops 2 | bytes 16 | tf_op jit(solution)/shard_map/psum | solution.py:58
  155.8 3.1 %broadcast_multiply_fusion = f32[2,1024,512]{2,1,0:T(8,128)S(1)} fusion(f32[2,1024,512]{2,1,0:T(8,128)} %get-tuple-element.21, f32[2]{0:T(128)S(1)} %add_rsqrt_fusion), kind=kLoop, calls=%fused_computation.7 | loop fusion | flops 1048576 | bytes 8388616 | tf_op jit(solution)/shard_map/mul | solution.py:60
  158.9 2.6 fusion.15
  161.5 0.4 copy-done.1
  161.9 0.0 all-gather.3.cloned.1.call-start
  162.0 4.5 %fusion.17 = (bf16[1024,512]{1,0:T(8,128)(2,1)}, f32[1024,512]{1,0:T(8,128)}) fusion(f32[1024,512]{1,0:T(8,128)} %param.14, f32[2,1024,512]{2,1,0:T(8,128)} %copy-done.1), kind=kLoop, calls=%fused_computation.30 | loop fusion | flops 1572864 | bytes 7340032 | tf_op jit(solution)/shard_map/convert_element_type | solution.py:64
  166.5 3.1 %copy.16 = f32[512,1024]{1,0:T(8,128)} copy(f32[512,1024]{0,1:T(8,128)} %get-tuple-element.15) | data formatting | bytes 4194304
  169.5 42.3 %all-gather.5.cloned.1.call-done = bf16[512,4096]{0,1:T(8,128)(2,1)} async-done(((bf16[512,1024]{0,1:T(8,128)(2,1)}), bf16[512,4096]{0,1:T(8,128)(2,1)}) %all-gather.5.cloned.1.call-update) | async-done | bytes 4194320 | tf_op jit(solution)/shard_map/all_gather | solution.py:65
  211.9 6.3 %copy.17 = bf16[512,4096]{1,0:T(8,128)(2,1)} copy(bf16[512,4096]{0,1:T(8,128)(2,1)} %all-gather.5.cloned.1.call-done) | data formatting | bytes 8388608
  218.2 48.0 %all-gather.3.cloned.1.call-done = bf16[4096,512]{1,0:T(8,128)(2,1)} async-done(((bf16[1024,512]{1,0:T(8,128)(2,1)}), bf16[4096,512]{1,0:T(8,128)(2,1)}) %all-gather.3.cloned.1.call-update) | async-done | bytes 4194320 | tf_op jit(solution)/shard_map/all_gather | solution.py:64
  266.2 4.5 %copy.22 = bf16[4096,512]{1,0:T(8,128)(2,1)} copy(bf16[4096,512]{1,0:T(8,128)(2,1)} %all-gather.3.cloned.1.call-done) | data formatting | bytes 8388608
  (19 shorter events, 0.2 us)
Async XLA Ops:
  7.2 1.6 copy-start
  7.2 66.9 %copy-start.5 = (bf16[672,512]{1,0:T(8,128)(2,1)S(1)}, bf16[672,512]{1,0:T(8,128)(2,1)}, u32[]{:S(2)}) copy-start(bf16[672,512]{1,0:T(8,128)(2,1)} %param.11) | copy-start | bytes 2064388
  7.2 66.9 %all-reduce.6.cloned.1.call-start = ((), (), s32[]{:S(2)}) async-start(), calls=%async_computation.3 | async-start | bytes 1572864 | tf_op jit(solution)/shard_map/psum | solution.py:46
  8.8 66.8 %copy-start.6 = (bf16[672,512]{1,0:T(8,128)(2,1)S(1)}, bf16[672,512]{1,0:T(8,128)(2,1)}, u32[]{:S(2)}) copy-start(bf16[672,512]{1,0:T(8,128)(2,1)} %param.10) | copy-start | bytes 2064388
  13.3 109.3 %all-reduce.4.cloned.1.call-start = ((), (), s32[]{:S(2)}) async-start(), calls=%async_computation | async-start | bytes 1048576 | tf_op jit(solution)/shard_map/psum | solution.py:53
  77.9 133.9 %all-gather.5.cloned.1.call-start = ((), (), s32[]{:S(2)}) async-start(), calls=%async_computation.2 | async-start | bytes 5242880 | tf_op jit(solution)/shard_map/all_gather | solution.py:65
  124.2 4.0 %copy-start.3 = (f32[2,128,512]{2,1,0:T(8,128)}, f32[2,128,512]{2,1,0:T(8,128)S(1)}, u32[]{:S(2)}) copy-start(f32[2,128,512]{2,1,0:T(8,128)S(1)} %get-tuple-element.33) | copy-start | bytes 1572868
  124.2 4.0 %copy-start.4 = (f32[2,128,512]{2,1,0:T(8,128)}, f32[2,128,512]{2,1,0:T(8,128)S(1)}, u32[]{:S(2)}) copy-start(f32[2,128,512]{2,1,0:T(8,128)S(1)} %get-tuple-element.32) | copy-start | bytes 1572868
  155.8 3.1 %copy-start.2 = (f32[512,1024]{0,1:T(8,128)S(1)}, f32[512,1024]{0,1:T(8,128)}, u32[]{:S(2)}) copy-start(f32[512,1024]{0,1:T(8,128)} %copy.15) | copy-start | bytes 6291460
  158.9 3.0 %copy-start.1 = (f32[2,1024,512]{2,1,0:T(8,128)}, f32[2,1024,512]{2,1,0:T(8,128)S(1)}, u32[]{:S(2)}) copy-start(f32[2,1024,512]{2,1,0:T(8,128)S(1)} %broadcast_multiply_fusion) | copy-start | bytes 12582916
  161.9 104.3 %all-gather.3.cloned.1.call-start = ((), (), s32[]{:S(2)}) async-start(), calls=%async_computation.1 | async-start | bytes 5242880 | tf_op jit(solution)/shard_map/all_gather | solution.py:64
Sparse Core Ops, SparseCore 0:
  13.4 60.6 all-reduce.5
  78.1 44.4 all-reduce.3
  162.0 49.7 all-gather.4
  213.6 52.5 all-gather.2
